TPU v7x, 256 devices: a whole 4x4x8 slice. The times are simulated.
256 devices in a mesh: ep: 16 (over y, x), tp: 16 (over z, core).
Axes of the slice: x: 4, y: 4, z: 8, core: 2. Of those that a mesh axis runs over, the one named last changes fastest.
Arguments:
- tokens: bfloat16 [256, 2048], P('ep', 'tp'), may hold values from -6 to 6
- key_cache: bfloat16 [256, 16, 1024, 128], P('ep', 'tp'), may hold values from -1700 to 1700
- value_cache: bfloat16 [256, 16, 1024, 128], P('ep', 'tp'), may hold values from -6 to 6
- gate_totals: float32 [256, 16, 1024], P('ep', 'tp'), as said below
- lengths: int32 [256], P('ep'), may hold values from 128 to 1024
- attn_gain: float32 [2048], replicated, may hold values from 0.1 to 1.9
- w_query: bfloat16 [2048, 2048], P(None, 'tp'), may hold values from -0.125 to 0.125
- w_key: bfloat16 [2048, 2048], P(None, 'tp'), may hold values from -0.125 to 0.125
- w_value: bfloat16 [2048, 2048], P(None, 'tp'), may hold values from -0.125 to 0.125
- w_forget: bfloat16 [2048, 16], replicated, may hold values from -0.125 to 0.125
- forget_bias: float32 [16], replicated, may hold values from -3 to 0
- w_attn_out: bfloat16 [2048, 2048], P('tp'), may hold values from -0.1875 to 0.1875
- moe_gain: float32 [2048], replicated, may hold values from 0.1 to 1.9
- group_ids: int32 [256, 1], P('ep'), may hold values from 0 to 15; in each aligned block of 16 rows (0 to 15, 16 to 31, ...) at most 2 rows name the same one
- inner_ids: int32 [256, 2], P('ep'), may hold values from 0 to 3, all different within a row
- group_prob: float32 [256], P('ep'), may hold values from 0.2 to 1
- pair_logits: float32 [256, 2], P('ep'), may hold values from -6 to 6
- w_expert_gate: bfloat16 [16, 2048, 2048], P('ep', None, 'tp'), may hold values from -0.125 to 0.125
- w_expert_up: bfloat16 [16, 2048, 2048], P('ep', None, 'tp'), may hold values from -0.125 to 0.125
- w_expert_down: bfloat16 [16, 2048, 2048], P('ep', 'tp'), may hold values from -0.375 to 0.375
- w_dense_in: bfloat16 [2048, 2048], P(None, 'tp'), may hold values from -0.125 to 0.125
- w_dense_out: bfloat16 [2048, 2048], P('tp'), may hold values from -0.1875 to 0.1875
- dense_gate: float32 [2048], P('tp'), may hold values from -2 to 2
Outputs:
- layer_output: bfloat16 [256, 2048], P('ep', 'tp')
- new_keys: bfloat16 [256, 16, 128], P('ep', 'tp')
- new_values: bfloat16 [256, 16, 128], P('ep', 'tp')
- new_gates: float32 [256, 16], P('ep', 'tp')
Inputs may be any that keep to these rules, and one draw needn't show every extreme that they name: `group_ids`: within the 16 sequences of each index of ep (aligned blocks of rows), no group is named by more than 2 sequences, a bound that some block reaches. `inner_ids`: each row names 2 different experts of its group. `gate_totals`: along positions the values of each sequence and head never rise.
All inputs are finite; a program needn't handle non-finite values.
Results may differ from a plain program's by a relative error of at most 0.011.
Values may be sent and summed in bfloat16 or wider, within the bound.
A program may use at most 64 MiB of HBM per device.

v0:
```python
import jax
import jax.numpy as jnp
from jax import lax
from jax.sharding import PartitionSpec as P

FFE = 512
EPG = 4
EPS = 1e-06
FLOOR = -1e30


def split_up(array, dim, size):
    dims = array.shape
    pieces = array.reshape(*dims[:dim], size, dims[dim] // size, *dims[dim + 1 :])
    return jnp.moveaxis(pieces, dim, 0)


def sum_at_owner(array, axis, dim):
    size = lax.axis_size(axis)
    pieces = lax.all_to_all(split_up(array, dim, size), axis, 0, 0, tiled=True)
    return jnp.sum(pieces, axis=0)


def joined_along(pieces, dim):
    dims = list(pieces.shape[1:])
    dims[dim] *= pieces.shape[0]
    return jnp.moveaxis(pieces, 0, dim).reshape(dims)


def copy_for_each(array, axis):
    copies = jnp.broadcast_to(array, (lax.axis_size(axis), *array.shape))
    return lax.all_to_all(copies, axis, split_axis=0, concat_axis=0, tiled=True)


def gathered_copies(array, axis, dim):
    return joined_along(copy_for_each(array, axis), dim)


def side_by_side(arrays, axis, split_dim, concat_dim, along):
    both = jnp.concatenate(arrays, axis=along)
    filled, at, gathered = (
        lax.all_to_all(both, axis, split_axis=split_dim, concat_axis=concat_dim, tiled=True),
        0,
        [],
    )
    for a in arrays:
        gathered.append(lax.slice_in_dim(filled, at, at + a.shape[along], axis=along))
        at += a.shape[along]
    return tuple(gathered)


def sent_together(arrays, axis, dim, along):
    widths = [a.shape[along] for a in arrays]
    both = jnp.concatenate(arrays, axis=along)
    filled = sum_at_owner(both, axis, dim)
    return tuple(jnp.split(filled, [sum(widths[:k]) for k in range(1, len(widths))], axis=along))


def norm_rows(row_data, gain_vec):
    values = row_data.astype(jnp.float32)
    factor = lax.rsqrt(jnp.mean(values * values, axis=-1, keepdims=True) + EPS)
    return (values * factor * gain_vec).astype(jnp.bfloat16)


def head_norm(values):
    factor = lax.rsqrt(jnp.mean(values * values, axis=-1, keepdims=True) + EPS)
    return (values * factor).astype(jnp.bfloat16)


def attend(queries, fresh_key, fresh_value, key_cache, value_cache, gate_totals, lengths, current):
    score_scale = queries.shape[-1] ** (-0.5)
    scores = (
        jnp.einsum("shd,shld->shl", queries, key_cache, preferred_element_type=jnp.float32)
        * score_scale
    )
    scores = scores + current[:, :, None] - gate_totals
    entry_indices = jnp.arange(key_cache.shape[2])
    live_mask = (entry_indices[None, :] < lengths[:, None])[:, None, :]
    scores = jnp.where(live_mask, scores, FLOOR)
    own_score = (
        jnp.sum(queries.astype(jnp.float32) * fresh_key.astype(jnp.float32), axis=-1) * score_scale
    )
    peak = jnp.maximum(jnp.max(scores, axis=-1), own_score)
    expo_terms = jnp.where(live_mask, jnp.exp(scores - peak[:, :, None]), 0.0)
    own_expo = jnp.exp(own_score - peak)
    denom_sum = jnp.sum(expo_terms, axis=-1) + own_expo
    weights = (expo_terms / denom_sum[:, :, None]).astype(jnp.bfloat16)
    own_weight = (own_expo / denom_sum).astype(jnp.bfloat16)
    attended = jnp.einsum("shl,shld->shd", weights, value_cache, preferred_element_type=jnp.float32)
    attended = attended + own_weight.astype(jnp.float32)[:, :, None] * fresh_value.astype(
        jnp.float32
    )
    return attended.astype(jnp.bfloat16)


def body(
    tokens,
    key_cache,
    value_cache,
    gate_totals,
    lengths,
    attn_gain,
    w_query,
    w_key,
    w_value,
    w_forget,
    forget_bias,
    w_attn_out,
    moe_gain,
    group_ids,
    inner_ids,
    group_prob,
    pair_logits,
    w_expert_gate,
    w_expert_up,
    w_expert_down,
    w_dense_in,
    w_dense_out,
    dense_gate,
):
    gathered = lax.all_gather(tokens, "tp", axis=1, tiled=True)
    normed = norm_rows(gathered, attn_gain)
    seq_count = gathered.shape[0]
    heads_dev = key_cache.shape[1]
    head_dim = key_cache.shape[3]

    def project(weight):
        return jnp.dot(normed, weight, preferred_element_type=jnp.float32).reshape(
            seq_count, heads_dev, head_dim
        )

    queries = head_norm(project(w_query))
    new_keys = head_norm(project(w_key))
    new_values = project(w_value).astype(jnp.bfloat16)
    first_head = lax.axis_index("tp") * heads_dev
    forget_cols = lax.dynamic_slice_in_dim(w_forget, first_head, heads_dev, 1)
    forget_shift = lax.dynamic_slice_in_dim(forget_bias, first_head, heads_dev, 0)
    log_gate = jax.nn.log_sigmoid(
        jnp.dot(normed, forget_cols, preferred_element_type=jnp.float32) + forget_shift
    )
    entry_indices = jnp.arange(gate_totals.shape[2])
    at_last = (entry_indices[None, :] == (lengths - 1)[:, None])[:, None, :]
    new_gates = jnp.sum(jnp.where(at_last, gate_totals, 0.0), axis=2) + log_gate
    attended = attend(
        queries, new_keys, new_values, key_cache, value_cache, gate_totals, lengths, new_gates
    )
    partial_value = jnp.dot(
        attended.reshape(seq_count, heads_dev * head_dim),
        w_attn_out,
        preferred_element_type=jnp.float32,
    )
    piece_sum = sum_at_owner(partial_value, "tp", 1)
    own_residual = (tokens.astype(jnp.float32) + piece_sum).astype(jnp.bfloat16)
    moe_in = norm_rows(gathered_copies(own_residual, "tp", 1), moe_gain)
    groups = lax.axis_size("ep")
    capacity = max(2, 2 * seq_count // groups)
    first_share = jax.nn.sigmoid(pair_logits[:, 0] - pair_logits[:, 1])
    pair_share = group_prob[:, None] * jnp.stack([first_share, 1.0 - first_share], axis=1)
    inner_range = jnp.arange(EPG)
    spread = jnp.sum(
        jnp.where(inner_ids[:, :, None] == inner_range[None, None, :], pair_share[:, :, None], 0.0),
        axis=1,
    ).astype(jnp.bfloat16)
    choose = (group_ids == jnp.arange(groups)[None, :]).astype(jnp.int32)
    before = jnp.cumsum(choose, axis=0) - choose
    slot_of = group_ids[:, 0] * capacity + jnp.sum(before * choose, axis=1)
    slot_ids = jnp.arange(groups * capacity)
    send_map = (slot_of[None, :] == slot_ids[:, None]).astype(jnp.bfloat16)
    send_weights = jnp.dot(send_map, spread, preferred_element_type=jnp.float32).astype(
        jnp.bfloat16
    )
    send_rows = jnp.dot(send_map, moe_in, preferred_element_type=jnp.float32).astype(jnp.bfloat16)
    recv_rows, recv_weights = side_by_side((send_rows, send_weights), "ep", 0, 0, 1)
    dense_hidden = jax.nn.silu(
        jnp.dot(moe_in, w_dense_in, preferred_element_type=jnp.float32)
    ).astype(jnp.bfloat16)
    dense_part = jnp.dot(dense_hidden, w_dense_out, preferred_element_type=jnp.float32)
    hidden_dev = w_expert_gate.shape[2]
    expert_index = lax.axis_index("tp") * hidden_dev // FFE
    route_col = jnp.sum(
        jnp.where(inner_range[None, :] == expert_index, recv_weights.astype(jnp.float32), 0.0),
        axis=1,
    )
    gate_pre = jnp.dot(recv_rows, w_expert_gate[0], preferred_element_type=jnp.float32)
    up_pre = jnp.dot(recv_rows, w_expert_up[0], preferred_element_type=jnp.float32)
    hidden = (jax.nn.silu(gate_pre) * up_pre * route_col[:, None]).astype(jnp.bfloat16)
    expert_part = jnp.dot(hidden, w_expert_down[0], preferred_element_type=jnp.float32)
    expert_sum, dense_sum = sent_together((expert_part, dense_part), "tp", 1, 0)
    returned = lax.all_to_all(
        expert_sum.astype(jnp.bfloat16), "ep", split_axis=0, concat_axis=0, tiled=True
    )
    expert_out = lax.dot_general(
        send_map, returned, (((0,), (0,)), ((), ())), preferred_element_type=jnp.float32
    )
    layer_output = (
        own_residual.astype(jnp.float32) + expert_out + jax.nn.sigmoid(dense_gate) * dense_sum
    )
    return (layer_output.astype(jnp.bfloat16), new_keys, new_values, new_gates)


def solution(mesh):
    placed = (
        P("ep", "tp"),
        P("ep", "tp", None, None),
        P("ep", "tp", None, None),
        P("ep", "tp", None),
        P("ep"),
        P(),
        P(None, "tp"),
        P(None, "tp"),
        P(None, "tp"),
        P(),
        P(),
        P("tp", None),
        P(),
        P("ep", None),
        P("ep", None),
        P("ep"),
        P("ep", None),
        P("ep", None, "tp"),
        P("ep", None, "tp"),
        P("ep", "tp", None),
        P(None, "tp"),
        P("tp", None),
        P("tp"),
    )
    return jax.shard_map(
        body,
        mesh=mesh,
        in_specs=placed,
        out_specs=(P("ep", "tp"), P("ep", "tp", None), P("ep", "tp", None), P("ep", "tp")),
        check_vma=False,
    )
```

profile of v0, /device:TPU:1, one launch (start us, length us, event | category | flops | bytes accessed | tf_op | source)
XLA Modules:
  0.0 108.0 jit_solution(13230268292263461012)
XLA Ops:
  0.7 21.8 %all_gather.3 = bf16[16,2048]{1,0:T(8,128)(2,1)S(1)} all-gather(bf16[16,128]{1,0:T(8,128)(2,1)} %param.23), channel_id=1, replica_groups=mesh['ep'=16,'tp'=16] {'tp'}, dimensions={1}, use_global_device_ids=true | all-gather | bytes 69632 | tf_op jit(solution)/shard_map/all_gather | solution.py:121
  22.7 1.4 %multiply_reduce_fusion.1 = (f32[16]{0:T(128)S(1)}, f32[16,128]{1,0:T(8,128)S(1)}) fusion(bf16[2048,128]{1,0:T(8,128)(2,1)} %param.30, bf16[16,2048]{1,0:T(8,128)(2,1)S(1)} %all_gather.3, f32[2048]{0:T(1024)} %param.28, f32[16]{0:T(128)S(1)} %add_rsqrt_fusion.3), kind=kOutput, calls=%fused_computation.71 | convolution fusion | flops 8523760 | bytes 606336 | tf_op jit(solution)/shard_map/dot_general | solution.py:128
  24.1 1.4 %multiply_reduce_fusion.2 = (f32[16]{0:T(128)S(1)}, f32[16,128]{1,0:T(8,128)S(1)}) fusion(bf16[2048,128]{1,0:T(8,128)(2,1)} %param.29, bf16[16,2048]{1,0:T(8,128)(2,1)S(1)} %all_gather.3, f32[2048]{0:T(1024)} %param.28, f32[16]{0:T(128)S(1)} %add_rsqrt_fusion.3), kind=kOutput, calls=%fused_computation.74 | convolution fusion | flops 8523760 | bytes 606336 | tf_op jit(solution)/shard_map/dot_general | solution.py:128
  25.5 0.7 broadcast_add_fusion
  26.2 0.8 fusion.59
  27.0 3.4 %fusion.2 = f32[16,1,1024]{2,1,0:T(1,128)S(1)} fusion(bf16[16,1,1024,128]{3,2,1,0:T(8,128)(2,1)} %param.24, bf16[16,128,1]{1,0,2:T(8,128)(2,1)S(1)} %get-tuple-element.10), kind=kOutput, calls=%fused_computation.2 | convolution fusion | flops 4194304 | bytes 4263936 | tf_op jit(solution)/shard_map/shd,shld->shl/dot_general | solution.py:73
  30.4 0.6 dynamic_slice.7
  31.3 1.6 %fusion.51 = f32[16]{0:T(128)S(1)} fusion(f32[16]{0:T(128)S(1)} %fusion.29, bf16[2048,16]{0,1:T(8,128)(2,1)} %param.32, s32[]{:T(128)S(6)} %select_n.34, f32[]{:T(128)} %bitcast.4, bf16[16,2048]{1,0:T(8,128)(2,1)S(1)} %all_gather.3, f32[2048]{0:T(1024)S(1)} %copy-done.8, f32[16]{0:T(128)S(1)} %add_rsqrt_fusion.3), kind=kOutput, calls=%fused_computation.85 | convolution fusion | flops 196768 | bytes 82628 | tf_op jit(solution)/shard_map/dot_general | solution.py:139
  34.3 3.0 %fusion = f32[16,1,128]{2,1,0:T(1,128)S(1)} fusion(bf16[16,1,1024,128]{3,2,1,0:T(8,128)(2,1)} %param.25, f32[16]{0:T(128)S(1)} %get-tuple-element.12, f32[16,1,1024]{2,1,0:T(1,128)S(1)} %get-tuple-element.7, f32[16]{0:T(128)S(1)} %multiply_maximum_fusion, s32[16]{0:T(128)S(1)} %copy-done.12), kind=kOutput, calls=%fused_computation | convolution fusion | flops 4276224 | bytes 4268224 | tf_op jit(solution)/shard_map/shl,shld->shd/dot_general | solution.py:89
  37.3 0.9 convolution_bitcast_fusion
  38.3 3.8 %all-to-all-start = ((f32[16,16,128]{2,1,0:T(8,128)}), f32[16,16,128]{2,1,0:T(8,128)S(1)}, u32[]{:S(2)}, u32[]{:S(2)}) async-start(f32[16,16,128]{2,1,0:T(8,128)} %convolution_bitcast_fusion), calls=%async_computation | async-start | bytes 262144 | tf_op jit(solution)/shard_map/all_to_all | solution.py:20
  42.5 8.5 %all-to-all-done = f32[16,16,128]{2,1,0:T(8,128)S(1)} async-done(((f32[16,16,128]{2,1,0:T(8,128)}), f32[16,16,128]{2,1,0:T(8,128)S(1)}, u32[]{:S(2)}, u32[]{:S(2)}) %all-to-all-start) | async-done | bytes 131104 | tf_op jit(solution)/shard_map/all_to_all | solution.py:20
  51.0 0.6 broadcast_in_dim.32
  51.6 3.4 %all-to-all-start.1 = ((bf16[16,16,128]{2,1,0:T(8,128)(2,1)}), bf16[16,16,128]{2,1,0:T(8,128)(2,1)S(1)}, u32[]{:S(2)}, u32[]{:S(2)}) async-start(bf16[16,16,128]{2,1,0:T(8,128)(2,1)} %broadcast_in_dim.32), calls=%async_computation.1 | async-start | bytes 131072 | tf_op jit(solution)/shard_map/all_to_all | solution.py:32
  55.3 7.2 %all-to-all-done.1 = bf16[16,16,128]{2,1,0:T(8,128)(2,1)S(1)} async-done(((bf16[16,16,128]{2,1,0:T(8,128)(2,1)}), bf16[16,16,128]{2,1,0:T(8,128)(2,1)S(1)}, u32[]{:S(2)}, u32[]{:S(2)}) %all-to-all-start.1) | async-done | bytes 65568 | tf_op jit(solution)/shard_map/all_to_all | solution.py:32
  62.9 0.7 all_to_all.27
  63.6 6.8 %all-to-all-start.2 = ((bf16[16,2,2052]{2,1,0:T(2,128)(2,1)}), bf16[16,2,2052]{2,1,0:T(2,128)(2,1)S(1)}, u32[]{:S(2)}, u32[]{:S(2)}) async-start(bf16[16,2,2052]{2,1,0:T(2,128)(2,1)} %all_to_all.27), calls=%async_computation.2 | async-start | bytes 278528 | tf_op jit(solution)/shard_map/all_to_all | solution.py:42
  70.4 0.4 fusion.44
  70.8 6.4 %all-to-all-done.2 = bf16[16,2,2052]{2,1,0:T(2,128)(2,1)S(1)} async-done(((bf16[16,2,2052]{2,1,0:T(2,128)(2,1)}), bf16[16,2,2052]{2,1,0:T(2,128)(2,1)S(1)}, u32[]{:S(2)}, u32[]{:S(2)}) %all-to-all-start.2) | async-done | bytes 131360 | tf_op jit(solution)/shard_map/all_to_all | solution.py:42
  78.1 18.6 %all_to_all.39 = f32[16,48,128]{2,1,0:T(8,128)S(1)} all-to-all(f32[16,48,128]{2,1,0:T(8,128)S(1)} %bitcast_bitcast_fusion), channel_id=1, replica_groups=mesh['ep'=16,'tp'=16] {'tp'}, dimensions={0} | all-to-all | bytes 786432 | tf_op jit(solution)/shard_map/all_to_all | solution.py:20
  96.8 0.6 split.15
  97.4 3.5 %all-to-all-start.4 = ((bf16[16,2,128]{2,1,0:T(2,128)(2,1)}), bf16[16,2,128]{2,1,0:T(2,128)(2,1)S(1)}, u32[]{:S(2)}, u32[]{:S(2)}) async-start(bf16[16,2,128]{2,1,0:T(2,128)(2,1)} %bitcast.19), calls=%async_computation.4 | async-start | bytes 16384 | tf_op jit(solution)/shard_map/all_to_all | solution.py:189
  100.9 6.3 %all-to-all-done.4 = bf16[16,2,128]{2,1,0:T(2,128)(2,1)S(1)} async-done(((bf16[16,2,128]{2,1,0:T(2,128)(2,1)}), bf16[16,2,128]{2,1,0:T(2,128)(2,1)S(1)}, u32[]{:S(2)}, u32[]{:S(2)}) %all-to-all-start.4) | async-done | bytes 8224 | tf_op jit(solution)/shard_map/all_to_all | solution.py:189
  107.3 0.8 fusion.8
  (74 shorter events, 3.7 us)
Async XLA Ops:
  0.6 77.0 %copy-start = (bf16[1,128,2048]{2,1,0:T(8,128)(2,1)S(1)}, bf16[1,128,2048]{2,1,0:T(8,128)(2,1)}, u32[]{:S(2)}) copy-start(bf16[1,128,2048]{2,1,0:T(8,128)(2,1)} %param.42) | copy-start | bytes 1572868
  0.6 30.7 %copy-start.8 = (f32[2048]{0:T(1024)S(1)}, f32[2048]{0:T(1024)}, u32[]{:S(2)}) copy-start(f32[2048]{0:T(1024)} %param.28) | copy-start | bytes 24580
  0.7 32.4 %copy-start.12 = (s32[16]{0:T(128)S(1)}, s32[16]{0:T(128)}, u32[]{:S(2)}) copy-start(s32[16]{0:T(128)} %param.27) | copy-start | bytes 196
  0.7 29.7 %copy-start.18 = (f32[16]{0:T(128)S(1)}, f32[16]{0:T(128)}, u32[]{:S(2)}) copy-start(f32[16]{0:T(128)} %param.33) | copy-start | bytes 196
  0.7 30.3 %copy-start.7 = (f32[16,1,1024]{2,1,0:T(1,128)S(1)}, f32[16,1,1024]{2,1,0:T(1,128)}, u32[]{:S(2)}) copy-start(f32[16,1,1024]{2,1,0:T(1,128)} %param.26) | copy-start | bytes 196612
  0.7 33.0 %copy-start.1 = (bf16[2048,128]{1,0:T(8,128)(2,1)S(1)}, bf16[2048,128]{1,0:T(8,128)(2,1)}, u32[]{:S(2)}) copy-start(bf16[2048,128]{1,0:T(8,128)(2,1)} %param.31) | copy-start | bytes 1572868
  0.7 33.3 %copy-start.2 = (bf16[128,2048]{1,0:T(8,128)(2,1)S(1)}, bf16[128,2048]{1,0:T(8,128)(2,1)}, u32[]{:S(2)}) copy-start(bf16[128,2048]{1,0:T(8,128)(2,1)} %param.34) | copy-start | bytes 1572868
  30.4 11.7 %copy-start.13 = (s32[16,1]{0,1:T(1,128)S(1)}, s32[16,1]{0,1:T(1,128)}, u32[]{:S(2)}) copy-start(s32[16,1]{0,1:T(1,128)} %param.36) | copy-start | bytes 196
  30.4 12.0 %copy-start.15 = (f32[16,2]{0,1:T(2,128)S(1)}, f32[16,2]{0,1:T(2,128)}, u32[]{:S(2)}) copy-start(f32[16,2]{0,1:T(2,128)} %param.39) | copy-start | bytes 388
  30.4 12.0 %copy-start.17 = (f32[16]{0:T(128)S(1)}, f32[16]{0:T(128)}, u32[]{:S(2)}) copy-start(f32[16]{0:T(128)} %param.38) | copy-start | bytes 196
  30.4 12.1 %copy-start.14 = (s32[16,2]{0,1:T(2,128)S(1)}, s32[16,2]{0,1:T(2,128)}, u32[]{:S(2)}) copy-start(s32[16,2]{0,1:T(2,128)} %param.37) | copy-start | bytes 388
  30.4 20.6 %copy-start.11 = (bf16[16,128]{1,0:T(8,128)(2,1)S(1)}, bf16[16,128]{1,0:T(8,128)(2,1)}, u32[]{:S(2)}) copy-start(bf16[16,128]{1,0:T(8,128)(2,1)} %param.23) | copy-start | bytes 12292
  30.4 32.2 %copy-start.9 = (f32[2048]{0:T(1024)S(1)}, f32[2048]{0:T(1024)}, u32[]{:S(2)}) copy-start(f32[2048]{0:T(1024)} %param.35) | copy-start | bytes 24580
  32.9 29.9 %copy-start.16 = (f32[16]{0:T(128)}, f32[16]{0:T(128)S(1)}, u32[]{:S(2)}) copy-start(f32[16]{0:T(128)S(1)} %fusion.51) | copy-start | bytes 196
  34.0 36.8 %copy-start.10 = (bf16[16,128]{1,0:T(8,128)(2,1)}, bf16[16,128]{1,0:T(8,128)(2,1)S(1)}, u32[]{:S(2)}) copy-start(bf16[16,128]{1,0:T(8,128)(2,1)S(1)} %convolution_convert_fusion.1) | copy-start | bytes 12292
  34.0 36.4 %copy-start.3 = (bf16[128,2048]{1,0:T(8,128)(2,1)S(1)}, bf16[128,2048]{1,0:T(8,128)(2,1)}, u32[]{:S(2)}) copy-start(bf16[128,2048]{1,0:T(8,128)(2,1)} %param.44) | copy-start | bytes 1572868
  34.0 36.4 %copy-start.4 = (bf16[2048,128]{1,0:T(8,128)(2,1)S(1)}, bf16[2048,128]{1,0:T(8,128)(2,1)}, u32[]{:S(2)}) copy-start(bf16[2048,128]{1,0:T(8,128)(2,1)} %param.43) | copy-start | bytes 1572868
  34.3 43.2 %copy-start.5 = (bf16[1,2048,128]{2,1,0:T(8,128)(2,1)S(1)}, bf16[1,2048,128]{2,1,0:T(8,128)(2,1)}, u32[]{:S(2)}) copy-start(bf16[1,2048,128]{2,1,0:T(8,128)(2,1)} %param.40) | copy-start | bytes 1572868
  34.3 43.4 %copy-start.6 = (bf16[1,2048,128]{2,1,0:T(8,128)(2,1)S(1)}, bf16[1,2048,128]{2,1,0:T(8,128)(2,1)}, u32[]{:S(2)}) copy-start(bf16[1,2048,128]{2,1,0:T(8,128)(2,1)} %param.41) | copy-start | bytes 1572868
  37.3 63.6 %copy-start.19 = (f32[128]{0:T(128)S(1)}, f32[128]{0:T(128)}, u32[]{:S(2)}) copy-start(f32[128]{0:T(128)} %param.45) | copy-start | bytes 1540
  38.3 12.7 %all-to-all-start = ((f32[16,16,128]{2,1,0:T(8,128)}), f32[16,16,128]{2,1,0:T(8,128)S(1)}, u32[]{:S(2)}, u32[]{:S(2)}) async-start(f32[16,16,128]{2,1,0:T(8,128)} %convolution_bitcast_fusion), calls=%async_computation | async-start | bytes 262144 | tf_op jit(solution)/shard_map/all_to_all | solution.py:20
  51.6 10.9 %all-to-all-start.1 = ((bf16[16,16,128]{2,1,0:T(8,128)(2,1)}), bf16[16,16,128]{2,1,0:T(8,128)(2,1)S(1)}, u32[]{:S(2)}, u32[]{:S(2)}) async-start(bf16[16,16,128]{2,1,0:T(8,128)(2,1)} %broadcast_in_dim.32), calls=%async_computation.1 | async-start | bytes 131072 | tf_op jit(solution)/shard_map/all_to_all | solution.py:32
  63.6 13.6 %all-to-all-start.2 = ((bf16[16,2,2052]{2,1,0:T(2,128)(2,1)}), bf16[16,2,2052]{2,1,0:T(2,128)(2,1)S(1)}, u32[]{:S(2)}, u32[]{:S(2)}) async-start(bf16[16,2,2052]{2,1,0:T(2,128)(2,1)} %all_to_all.27), calls=%async_computation.2 | async-start | bytes 278528 | tf_op jit(solution)/shard_map/all_to_all | solution.py:42
  97.4 9.9 %all-to-all-start.4 = ((bf16[16,2,128]{2,1,0:T(2,128)(2,1)}), bf16[16,2,128]{2,1,0:T(2,128)(2,1)S(1)}, u32[]{:S(2)}, u32[]{:S(2)}) async-start(bf16[16,2,128]{2,1,0:T(2,128)(2,1)} %bitcast.19), calls=%async_computation.4 | async-start | bytes 16384 | tf_op jit(solution)/shard_map/all_to_all | solution.py:189
where the time goes:
time: 109 us; the launch traced here: 108 us
  blocking collectives  40.5 us (37%)
  waiting for transfers between devices  28.5 us (26%)
  starting transfers between devices  17.4 us (16%)
  matrix products  14.1 us (13%)
  other arithmetic  3.35 us (3%)
  local copies, waits for them, and re-layouts  3.12 us (3%)
    all_gather x1, blocking collectives, body(): gathered = lax.all_gather(tokens, 'tp', axis=1, tiled=True)  21.8 us
    all_to_all x1, blocking collectives, sum_at_owner(): pieces = lax.all_to_all(split_up(array, dim, size), axis, 0, 0, tiled=True)  18.6 us
    all_to_all x1, waiting for transfers between devices, sum_at_owner(): pieces = lax.all_to_all(split_up(array, dim, size), axis, 0, 0, tiled=True)  8.5 us
    all_to_all x1, waiting for transfers between devices, copy_for_each(): return lax.all_to_all(copies, axis, split_axis=0, concat_axis=0, tiled=True)  7.21 us
    all_to_all x1, starting transfers between devices, side_by_side(): lax.all_to_all(both, axis, split_axis=split_dim, concat_axis=concat_dim,...  6.75 us
    all_to_all x1, waiting for transfers between devices, side_by_side(): lax.all_to_all(both, axis, split_axis=split_dim, concat_axis=concat_dim,...  6.44 us
    all_to_all x1, waiting for transfers between devices, body(): lax.all_to_all(expert_sum.astype(jnp.bfloat16), 'ep', split_axis=0, conca...  6.35 us
    all_to_all x1, starting transfers between devices, sum_at_owner(): pieces = lax.all_to_all(split_up(array, dim, size), axis, 0, 0, tiled=True)  3.81 us
  transfers between devices with their start and end apart: 4, of which 4 were waited for; matrix products, arithmetic and copies ran while one was open for 1% of the time, Pallas kernels for 0%

commit v1 on v0

--- a/solution.py
+++ b/solution.py
@@ -118,7 +118,10 @@
     w_dense_out,
     dense_gate,
 ):
-    gathered = lax.all_gather(tokens, "tp", axis=1, tiled=True)
+    count = lax.axis_size("tp")
+    blocks = jnp.stack([tokens for _ in range(count)])
+    blocks = lax.all_to_all(blocks, "tp", split_axis=0, concat_axis=0)
+    gathered = jnp.concatenate(blocks, axis=1)
     normed = norm_rows(gathered, attn_gain)
     seq_count = gathered.shape[0]
     heads_dev = key_cache.shape[1]

time: 109 us -> 105 us (0.963)
  blocking collectives: 40.5 us -> 18.6 us
  starting transfers between devices: 17.4 us -> 30.5 us
  other arithmetic: 3.35 us -> 6.91 us
  local copies, waits for them, and re-layouts: 3.12 us -> 6.18 us
  matrix products: 14.1 us -> 12.1 us
    all_gather x1 -> x0, blocking collectives: 21.8 us -> none  [body(): gathered = lax.all_gather(tokens, 'tp', axis=1, tiled=True)]
    all_to_all x0 -> x1, starting transfers between devices: none -> 9.97 us  [body(): blocks = lax.all_to_all(blocks, 'tp', split_axis=0, concat_axis=0)]
    all_to_all x1, starting transfers between devices: 3.81 us -> 6.86 us  [sum_at_owner(): pieces = lax.all_to_all(split_up(array, dim, size), axis, 0, 0, tiled=True)]
    dot_general x1, matrix products: 2.99 us -> 0.72 us  [attend(): jnp.einsum('shl,shld->shd', weights, value_cache, preferred_element_type=...]
    another operation x0 -> x1, local copies, waits for them, and re-layouts: none -> 1.38 us  [body(): blocks = jnp.stack([tokens for _ in range(count)])]
  transfers between devices with their start and end apart: 4 -> 5, of which waited for: 4 -> 5; matrix products, arithmetic and copies ran while one was open for 1% -> 8% of each run, Pallas kernels for 0% -> 0%
where the time goes in v1:
time: 105 us
  starting transfers between devices  30.5 us (29%)
  waiting for transfers between devices  29.2 us (28%)
  blocking collectives  18.6 us (18%)
  matrix products  12.1 us (12%)
  other arithmetic  6.91 us (7%)
  local copies, waits for them, and re-layouts  6.18 us (6%)
    all_to_all x1, blocking collectives, sum_at_owner(): pieces = lax.all_to_all(split_up(array, dim, size), axis, 0, 0, tiled=True)  18.6 us
    all_to_all x1, starting transfers between devices, body(): blocks = lax.all_to_all(blocks, 'tp', split_axis=0, concat_axis=0)  9.97 us
    all_to_all x1, waiting for transfers between devices, sum_at_owner(): pieces = lax.all_to_all(split_up(array, dim, size), axis, 0, 0, tiled=True)  8.84 us
    all_to_all x1, waiting for transfers between devices, copy_for_each(): return lax.all_to_all(copies, axis, split_axis=0, concat_axis=0, tiled=True)  7.21 us
    all_to_all x1, starting transfers between devices, sum_at_owner(): pieces = lax.all_to_all(split_up(array, dim, size), axis, 0, 0, tiled=True)  6.86 us
    all_to_all x1, starting transfers between devices, side_by_side(): lax.all_to_all(both, axis, split_axis=split_dim, concat_axis=concat_dim,...  6.75 us
    all_to_all x1, waiting for transfers between devices, side_by_side(): lax.all_to_all(both, axis, split_axis=split_dim, concat_axis=concat_dim,...  6.44 us
    all_to_all x1, waiting for transfers between devices, body(): lax.all_to_all(expert_sum.astype(jnp.bfloat16), 'ep', split_axis=0, conca...  6.35 us
  transfers between devices with their start and end apart: 5, of which 5 were waited for; matrix products, arithmetic and copies ran while one was open for 8% of the time, Pallas kernels for 0%

profile of v1, /device:TPU:1, one launch (start us, length us, event | category | flops | bytes accessed | tf_op | source)
XLA Modules:
  0.0 104.5 jit_solution(7083762711332940347)
XLA Ops:
  0.7 1.4 %stack.4 = bf16[16,16,128]{2,1,0:T(8,128)(2,1)} broadcast(bf16[16,128]{1,0:T(8,128)(2,1)} %param.23), dimensions={1,2} | broadcast | bytes 69632 | tf_op jit(solution)/shard_map/stack | solution.py:122
  2.1 10.0 %all-to-all-start = ((bf16[16,16,128]{2,1,0:T(8,128)(2,1)}), bf16[16,16,128]{2,1,0:T(8,128)(2,1)S(1)}, u32[]{:S(2)}, u32[]{:S(2)}) async-start(bf16[16,16,128]{2,1,0:T(8,128)(2,1)} %stack.4), calls=%async_computation | async-start | bytes 131072 | tf_op jit(solution)/shard_map/all_to_all | solution.py:123
  12.7 1.3 %copy.59 = bf16[2048,128]{1,0:T(8,128)(2,1)S(1)} copy(bf16[2048,128]{0,1:T(8,128)(2,1)} %bitcast.129) | data formatting | bytes 1048576 | tf_op jit(solution)/shard_map/dot_general | solution.py:150
  14.0 0.7 fusion.47
  14.8 0.8 select_reduce_fusion.1
  15.6 0.8 broadcast_subtract_fusion
  16.4 1.2 %dynamic_slice.7 = f32[1]{0:T(128)} dynamic-slice(f32[16]{0:T(128)} %param.33, s32[]{:T(128)S(6)} %select_n.34), dynamic_slice_sizes={1} | dynamic-slice | bytes 12 | tf_op jit(solution)/shard_map/dynamic_slice | solution.py:140
  18.3 1.1 %fusion.34 = f32[16]{0:T(128)S(1)} fusion(f32[16,1,1024]{2,1,0:T(1,128)} %param.26, s32[16]{0:T(128)S(1)} %broadcast_add_fusion), kind=kLoop, calls=%fused_computation.53 | loop fusion | flops 49136 | bytes 65664 | tf_op jit(solution)/shard_map/reduce_sum | solution.py:146
  19.9 1.6 %multiply_reduce_fusion.1 = (f32[16]{0:T(128)S(1)}, f32[16,128]{1,0:T(8,128)S(1)}) fusion(bf16[2048,128]{1,0:T(8,128)(2,1)} %param.30, f32[2048]{0:T(1024)} %param.28, f32[16]{0:T(128)S(1)} %add_rsqrt_fusion.3, bf16[16,16,128]{2,1,0:T(8,128)(2,1)S(1)} %all-to-all-done), kind=kOutput, calls=%fused_computation.78 | convolution fusion | flops 8523760 | bytes 606336 | tf_op jit(solution)/shard_map/dot_general | solution.py:131
  21.5 1.4 %multiply_reduce_fusion.2 = (f32[16]{0:T(128)S(1)}, f32[16,128]{1,0:T(8,128)S(1)}) fusion(bf16[2048,128]{1,0:T(8,128)(2,1)} %param.29, f32[2048]{0:T(1024)} %param.28, f32[16]{0:T(128)S(1)} %add_rsqrt_fusion.3, bf16[16,16,128]{2,1,0:T(8,128)(2,1)S(1)} %all-to-all-done), kind=kOutput, calls=%fused_computation.81 | convolution fusion | flops 8523760 | bytes 606336 | tf_op jit(solution)/shard_map/dot_general | solution.py:131
  22.9 0.8 fusion.66
  23.7 3.4 %fusion.2 = f32[16,1,1024]{2,1,0:T(1,128)S(1)} fusion(bf16[16,1,1024,128]{3,2,1,0:T(8,128)(2,1)} %param.24, bf16[16,128,1]{1,0,2:T(8,128)(2,1)S(1)} %get-tuple-element.10), kind=kOutput, calls=%fused_computation.2 | convolution fusion | flops 4194304 | bytes 4263936 | tf_op jit(solution)/shard_map/shd,shld->shl/dot_general | solution.py:73
  27.2 1.7 %fusion.56 = f32[16]{0:T(128)S(1)} fusion(f32[16]{0:T(128)S(1)} %fusion.34, bf16[2048,16]{0,1:T(8,128)(2,1)} %param.32, s32[]{:T(128)S(6)} %select_n.34, f32[]{:T(128)} %bitcast.7, bf16[16,16,128]{2,1,0:T(8,128)(2,1)S(1)} %all-to-all-done, f32[16,128]{1,0:T(8,128)S(1)} %bitcast.130, f32[16]{0:T(128)S(1)} %add_rsqrt_fusion.3), kind=kOutput, calls=%fused_computation.92 | convolution fusion | flops 196768 | bytes 82628 | tf_op jit(solution)/shard_map/dot_general | solution.py:142
  30.7 0.9 convolution_bitcast_fusion
  31.7 6.9 %all-to-all-start.1 = ((f32[16,16,128]{2,1,0:T(8,128)}), f32[16,16,128]{2,1,0:T(8,128)S(1)}, u32[]{:S(2)}, u32[]{:S(2)}) async-start(f32[16,16,128]{2,1,0:T(8,128)} %convolution_bitcast_fusion), calls=%async_computation.1 | async-start | bytes 262144 | tf_op jit(solution)/shard_map/all_to_all | solution.py:20
  38.6 8.8 %all-to-all-done.1 = f32[16,16,128]{2,1,0:T(8,128)S(1)} async-done(((f32[16,16,128]{2,1,0:T(8,128)}), f32[16,16,128]{2,1,0:T(8,128)S(1)}, u32[]{:S(2)}, u32[]{:S(2)}) %all-to-all-start.1) | async-done | bytes 131104 | tf_op jit(solution)/shard_map/all_to_all | solution.py:20
  48.1 3.4 %all-to-all-start.2 = ((bf16[16,16,128]{2,1,0:T(8,128)(2,1)}), bf16[16,16,128]{2,1,0:T(8,128)(2,1)S(1)}, u32[]{:S(2)}, u32[]{:S(2)}) async-start(bf16[16,16,128]{2,1,0:T(8,128)(2,1)} %broadcast_in_dim.32), calls=%async_computation.2 | async-start | bytes 131072 | tf_op jit(solution)/shard_map/all_to_all | solution.py:32
  51.7 7.2 %all-to-all-done.2 = bf16[16,16,128]{2,1,0:T(8,128)(2,1)S(1)} async-done(((bf16[16,16,128]{2,1,0:T(8,128)(2,1)}), bf16[16,16,128]{2,1,0:T(8,128)(2,1)S(1)}, u32[]{:S(2)}, u32[]{:S(2)}) %all-to-all-start.2) | async-done | bytes 65568 | tf_op jit(solution)/shard_map/all_to_all | solution.py:32
  60.0 6.8 %all-to-all-start.3 = ((bf16[16,2,2052]{2,1,0:T(2,128)(2,1)}), bf16[16,2,2052]{2,1,0:T(2,128)(2,1)S(1)}, u32[]{:S(2)}, u32[]{:S(2)}) async-start(bf16[16,2,2052]{2,1,0:T(2,128)(2,1)} %all_to_all.31), calls=%async_computation.3 | async-start | bytes 278528 | tf_op jit(solution)/shard_map/all_to_all | solution.py:42
  67.3 6.4 %all-to-all-done.3 = bf16[16,2,2052]{2,1,0:T(2,128)(2,1)S(1)} async-done(((bf16[16,2,2052]{2,1,0:T(2,128)(2,1)}), bf16[16,2,2052]{2,1,0:T(2,128)(2,1)S(1)}, u32[]{:S(2)}, u32[]{:S(2)}) %all-to-all-start.3) | async-done | bytes 131360 | tf_op jit(solution)/shard_map/all_to_all | solution.py:42
  74.6 18.6 %all_to_all.44 = f32[16,48,128]{2,1,0:T(8,128)S(1)} all-to-all(f32[16,48,128]{2,1,0:T(8,128)S(1)} %bitcast_bitcast_fusion), channel_id=1, replica_groups=mesh['ep'=16,'tp'=16] {'tp'}, dimensions={0} | all-to-all | bytes 786432 | tf_op jit(solution)/shard_map/all_to_all | solution.py:20
  93.8 3.5 %all-to-all-start.5 = ((bf16[16,2,128]{2,1,0:T(2,128)(2,1)}), bf16[16,2,128]{2,1,0:T(2,128)(2,1)S(1)}, u32[]{:S(2)}, u32[]{:S(2)}) async-start(bf16[16,2,128]{2,1,0:T(2,128)(2,1)} %bitcast.22), calls=%async_computation.5 | async-start | bytes 16384 | tf_op jit(solution)/shard_map/all_to_all | solution.py:192
  97.4 6.3 %all-to-all-done.5 = bf16[16,2,128]{2,1,0:T(2,128)(2,1)S(1)} async-done(((bf16[16,2,128]{2,1,0:T(2,128)(2,1)}), bf16[16,2,128]{2,1,0:T(2,128)(2,1)S(1)}, u32[]{:S(2)}, u32[]{:S(2)}) %all-to-all-start.5) | async-done | bytes 8224 | tf_op jit(solution)/shard_map/all_to_all | solution.py:192
  103.7 0.8 fusion.8
  (70 shorter events, 7.6 us)
Async XLA Ops:
  0.6 73.5 %copy-start = (bf16[1,128,2048]{2,1,0:T(8,128)(2,1)S(1)}, bf16[1,128,2048]{2,1,0:T(8,128)(2,1)}, u32[]{:S(2)}) copy-start(bf16[1,128,2048]{2,1,0:T(8,128)(2,1)} %param.42) | copy-start | bytes 1572868
  0.6 28.4 %copy-start.11 = (s32[16]{0:T(128)S(1)}, s32[16]{0:T(128)}, u32[]{:S(2)}) copy-start(s32[16]{0:T(128)} %param.27) | copy-start | bytes 196
  0.7 28.4 %copy-start.6 = (f32[16,1,1024]{2,1,0:T(1,128)S(1)}, f32[16,1,1024]{2,1,0:T(1,128)}, u32[]{:S(2)}) copy-start(f32[16,1,1024]{2,1,0:T(1,128)} %param.26) | copy-start | bytes 196612
  0.7 26.5 %copy-start.7 = (f32[2048]{0:T(1024)S(1)}, f32[2048]{0:T(1024)}, u32[]{:S(2)}) copy-start(f32[2048]{0:T(1024)} %param.28) | copy-start | bytes 24580
  2.1 17.7 %all-to-all-start = ((bf16[16,16,128]{2,1,0:T(8,128)(2,1)}), bf16[16,16,128]{2,1,0:T(8,128)(2,1)S(1)}, u32[]{:S(2)}, u32[]{:S(2)}) async-start(bf16[16,16,128]{2,1,0:T(8,128)(2,1)} %stack.4), calls=%async_computation | async-start | bytes 131072 | tf_op jit(solution)/shard_map/all_to_all | solution.py:123
  19.8 9.9 %copy-start.15 = (bf16[16,1,1024,128]{3,2,1,0:T(8,128)(2,1)S(1)}, bf16[16,1,1024,128]{3,2,1,0:T(8,128)(2,1)}, u32[]{:S(2)}) copy-start(bf16[16,1,1024,128]{3,2,1,0:T(8,128)(2,1)} %param.25) | copy-start | bytes 12582916
  23.7 6.8 %copy-start.1 = (bf16[2048,128]{1,0:T(8,128)(2,1)S(1)}, bf16[2048,128]{1,0:T(8,128)(2,1)}, u32[]{:S(2)}) copy-start(bf16[2048,128]{1,0:T(8,128)(2,1)} %param.31) | copy-start | bytes 1572868
  27.2 11.4 %copy-start.13 = (s32[16,2]{0,1:T(2,128)S(1)}, s32[16,2]{0,1:T(2,128)}, u32[]{:S(2)}) copy-start(s32[16,2]{0,1:T(2,128)} %param.37) | copy-start | bytes 388
  27.2 11.4 %copy-start.12 = (s32[16,1]{0,1:T(1,128)S(1)}, s32[16,1]{0,1:T(1,128)}, u32[]{:S(2)}) copy-start(s32[16,1]{0,1:T(1,128)} %param.36) | copy-start | bytes 196
  27.2 20.3 %copy-start.10 = (bf16[16,128]{1,0:T(8,128)(2,1)S(1)}, bf16[16,128]{1,0:T(8,128)(2,1)}, u32[]{:S(2)}) copy-start(bf16[16,128]{1,0:T(8,128)(2,1)} %param.23) | copy-start | bytes 12292
  27.2 31.9 %copy-start.8 = (f32[2048]{0:T(1024)S(1)}, f32[2048]{0:T(1024)}, u32[]{:S(2)}) copy-start(f32[2048]{0:T(1024)} %param.35) | copy-start | bytes 24580
  27.2 39.6 %copy-start.2 = (bf16[128,2048]{1,0:T(8,128)(2,1)S(1)}, bf16[128,2048]{1,0:T(8,128)(2,1)}, u32[]{:S(2)}) copy-start(bf16[128,2048]{1,0:T(8,128)(2,1)} %param.44) | copy-start | bytes 1572868
  27.2 39.6 %copy-start.3 = (bf16[2048,128]{1,0:T(8,128)(2,1)S(1)}, bf16[2048,128]{1,0:T(8,128)(2,1)}, u32[]{:S(2)}) copy-start(bf16[2048,128]{1,0:T(8,128)(2,1)} %param.43) | copy-start | bytes 1572868
  28.9 38.3 %copy-start.14 = (f32[16]{0:T(128)}, f32[16]{0:T(128)S(1)}, u32[]{:S(2)}) copy-start(f32[16]{0:T(128)S(1)} %fusion.56) | copy-start | bytes 196
  29.7 44.2 %copy-start.4 = (bf16[1,2048,128]{2,1,0:T(8,128)(2,1)S(1)}, bf16[1,2048,128]{2,1,0:T(8,128)(2,1)}, u32[]{:S(2)}) copy-start(bf16[1,2048,128]{2,1,0:T(8,128)(2,1)} %param.40) | copy-start | bytes 1572868
  29.7 44.4 %copy-start.5 = (bf16[1,2048,128]{2,1,0:T(8,128)(2,1)S(1)}, bf16[1,2048,128]{2,1,0:T(8,128)(2,1)}, u32[]{:S(2)}) copy-start(bf16[1,2048,128]{2,1,0:T(8,128)(2,1)} %param.41) | copy-start | bytes 1572868
  30.7 73.8 %copy-start.9 = (bf16[16,128]{1,0:T(8,128)(2,1)}, bf16[16,128]{1,0:T(8,128)(2,1)S(1)}, u32[]{:S(2)}) copy-start(bf16[16,128]{1,0:T(8,128)(2,1)S(1)} %convolution_convert_fusion.1) | copy-start | bytes 12292
  30.7 66.6 %copy-start.16 = (f32[128]{0:T(128)S(1)}, f32[128]{0:T(128)}, u32[]{:S(2)}) copy-start(f32[128]{0:T(128)} %param.45) | copy-start | bytes 1540
  31.7 15.7 %all-to-all-start.1 = ((f32[16,16,128]{2,1,0:T(8,128)}), f32[16,16,128]{2,1,0:T(8,128)S(1)}, u32[]{:S(2)}, u32[]{:S(2)}) async-start(f32[16,16,128]{2,1,0:T(8,128)} %convolution_bitcast_fusion), calls=%async_computation.1 | async-start | bytes 262144 | tf_op jit(solution)/shard_map/all_to_all | solution.py:20
  48.1 10.9 %all-to-all-start.2 = ((bf16[16,16,128]{2,1,0:T(8,128)(2,1)}), bf16[16,16,128]{2,1,0:T(8,128)(2,1)S(1)}, u32[]{:S(2)}, u32[]{:S(2)}) async-start(bf16[16,16,128]{2,1,0:T(8,128)(2,1)} %broadcast_in_dim.32), calls=%async_computation.2 | async-start | bytes 131072 | tf_op jit(solution)/shard_map/all_to_all | solution.py:32
  60.0 13.6 %all-to-all-start.3 = ((bf16[16,2,2052]{2,1,0:T(2,128)(2,1)}), bf16[16,2,2052]{2,1,0:T(2,128)(2,1)S(1)}, u32[]{:S(2)}, u32[]{:S(2)}) async-start(bf16[16,2,2052]{2,1,0:T(2,128)(2,1)} %all_to_all.31), calls=%async_computation.3 | async-start | bytes 278528 | tf_op jit(solution)/shard_map/all_to_all | solution.py:42
  93.8 9.9 %all-to-all-start.5 = ((bf16[16,2,128]{2,1,0:T(2,128)(2,1)}), bf16[16,2,128]{2,1,0:T(2,128)(2,1)S(1)}, u32[]{:S(2)}, u32[]{:S(2)}) async-start(bf16[16,2,128]{2,1,0:T(2,128)(2,1)} %bitcast.22), calls=%async_computation.5 | async-start | bytes 16384 | tf_op jit(solution)/shard_map/all_to_all | solution.py:192
